TPU v7x, 32 devices: a whole 2x2x4 slice. The times are simulated.
32 devices in a mesh: fs: 16 (over z, y, core), tp: 2 (over x).
Axes of the slice: x: 2, y: 2, z: 4, core: 2. Of those that a mesh axis runs over, the one named last changes fastest.
Arguments:
- inputs: bfloat16 [16384, 3072], P('fs'), may hold values from -6 to 6
- query_cot: bfloat16 [16384, 768], P('fs', 'tp'), may hold values from -0.046875 to 0.046875
- value_cot: bfloat16 [16384, 1536], P('fs', 'tp'), may hold values from -0.046875 to 0.046875
- query_factor: bfloat16 [3072, 192], P('fs'), may hold values from -0.109375 to 0.109375
- value_factor: bfloat16 [3072, 192], P('fs'), may hold values from -0.109375 to 0.109375
- query_weight: float32 [3072, 768], P('fs', 'tp'), may hold values from -0.109375 to 0.109375
- value_weight: float32 [3072, 1536], P('fs', 'tp'), may hold values from -0.109375 to 0.109375
- query_first: float32 [192, 768], P('fs', 'tp'), may hold values from -1.6 to 1.6
- query_second: float32 [192, 768], P('fs', 'tp'), may hold values from 0.002 to 0.05
- value_first: float32 [192, 1536], P('fs', 'tp'), may hold values from -1.6 to 1.6
- value_second: float32 [192, 1536], P('fs', 'tp'), may hold values from 0.002 to 0.05
Outputs:
- step_q: float32 [3072, 768], P('fs', 'tp')
- step_v: float32 [3072, 1536], P('fs', 'tp')
- new_q: float32 [3072, 768], P('fs', 'tp')
- new_v: float32 [3072, 1536], P('fs', 'tp')
- first_q: float32 [192, 768], P('fs', 'tp')
- second_q: float32 [192, 768], P('fs', 'tp')
- first_v: float32 [192, 1536], P('fs', 'tp')
- second_v: float32 [192, 1536], P('fs', 'tp')
- copy_q: bfloat16 [3072, 768], P(None, 'tp')
- copy_v: bfloat16 [3072, 1536], P(None, 'tp')
All inputs are finite; a program needn't handle non-finite values.
Results may differ from a plain program's by a relative error of at most 0.0041.
Values may be sent and summed in bfloat16 or wider, within the bound.
A program may use at most 64 MiB of HBM per device.

v0:
```python
import jax
import jax.numpy as jnp
from jax import lax
from jax.sharding import PartitionSpec as P

first_decay = 0.9
second_decay = 0.99
small_eps = 1e-08
learn_rate = 0.01


def moments(old_first, old_second, gradient):
    first = first_decay * old_first + (1.0 - first_decay) * gradient
    second = second_decay * old_second + (1.0 - second_decay) * gradient * gradient
    unit = first / (jnp.sqrt(second) + small_eps)
    return (first, second, unit)


def on_device(
    inputs,
    query_cot,
    value_cot,
    query_factor,
    value_factor,
    query_weight,
    value_weight,
    query_first,
    query_second,
    value_first,
    value_second,
):
    rank_cols = query_factor.shape[1]
    q_cols = query_cot.shape[1]
    v_cols = value_cot.shape[1]
    own_rows = query_first.shape[0]
    entries = rank_cols * (q_cols + v_cols) * lax.axis_size("tp")
    full_qf, full_vf = (
        lax.all_gather(query_factor, "fs", axis=0, tiled=True),
        lax.all_gather(value_factor, "fs", axis=0, tiled=True),
    )
    sum_q = jnp.dot(inputs, full_qf, preferred_element_type=jnp.float32)
    sum_v = jnp.dot(inputs, full_vf, preferred_element_type=jnp.float32)
    proj_q = sum_q.astype(jnp.bfloat16)
    proj_v = sum_v.astype(jnp.bfloat16)
    term_q = lax.dot_general(
        proj_q, query_cot, (((0,), (0,)), ((), ())), preferred_element_type=jnp.float32
    )
    term_v = lax.dot_general(
        proj_v, value_cot, (((0,), (0,)), ((), ())), preferred_element_type=jnp.float32
    )
    full_sums = lax.psum(jnp.concatenate([term_q, term_v], axis=1), "fs")
    stacked = (
        lax.all_gather(query_first, "fs", axis=0, tiled=True),
        lax.all_gather(query_second, "fs", axis=0, tiled=True),
        lax.all_gather(value_first, "fs", axis=0, tiled=True),
        lax.all_gather(value_second, "fs", axis=0, tiled=True),
    )
    all_first_q, all_second_q, unit_q = moments(stacked[0], stacked[1], full_sums[:, :q_cols])
    all_first_v, all_second_v, unit_v = moments(stacked[2], stacked[3], full_sums[:, q_cols:])
    norm_total = lax.psum(jnp.sum(unit_q * unit_q) + jnp.sum(unit_v * unit_v), "tp")
    step_scale = lax.rsqrt(norm_total / entries + 1e-06)
    whole_q = (step_scale * unit_q).astype(jnp.bfloat16)
    whole_v = (step_scale * unit_v).astype(jnp.bfloat16)
    row_begin = lax.axis_index("fs") * own_rows
    first_q = lax.dynamic_slice_in_dim(all_first_q, row_begin, own_rows, 0)
    second_q = lax.dynamic_slice_in_dim(all_second_q, row_begin, own_rows, 0)
    first_v = lax.dynamic_slice_in_dim(all_first_v, row_begin, own_rows, 0)
    second_v = lax.dynamic_slice_in_dim(all_second_v, row_begin, own_rows, 0)
    step_q = jnp.dot(query_factor, whole_q, preferred_element_type=jnp.float32)
    step_v = jnp.dot(value_factor, whole_v, preferred_element_type=jnp.float32)
    new_q = query_weight - learn_rate * step_q
    new_v = value_weight - learn_rate * step_v
    copy_q, copy_v = (
        lax.all_gather(new_q.astype(jnp.bfloat16), "fs", axis=0, tiled=True),
        lax.all_gather(new_v.astype(jnp.bfloat16), "fs", axis=0, tiled=True),
    )
    return (step_q, step_v, new_q, new_v, first_q, second_q, first_v, second_v, copy_q, copy_v)


def solution(mesh):
    in_specs = (
        P("fs", None),
        P("fs", "tp"),
        P("fs", "tp"),
        P("fs", None),
        P("fs", None),
        P("fs", "tp"),
        P("fs", "tp"),
        P("fs", "tp"),
        P("fs", "tp"),
        P("fs", "tp"),
        P("fs", "tp"),
    )
    out_specs = (
        P("fs", "tp"),
        P("fs", "tp"),
        P("fs", "tp"),
        P("fs", "tp"),
        P("fs", "tp"),
        P("fs", "tp"),
        P("fs", "tp"),
        P("fs", "tp"),
        P(None, "tp"),
        P(None, "tp"),
    )
    return jax.shard_map(
        on_device, mesh=mesh, in_specs=in_specs, out_specs=out_specs, check_vma=False
    )
```

profile of v0, /device:TPU:0, one launch (start us, length us, event | category | flops | bytes accessed | tf_op | source)
XLA Modules:
  0.0 321.6 jit_solution(11538157095303594677)
XLA Ops:
  8.0 0.7 all-gather.9.cloned.1.call-update
  8.7 24.6 %all-gather = f32[16,12,384]{2,1,0:T(8,128)S(1)} all-gather(f32[1,12,384]{2,1,0:T(8,128)} %bitcast.18), channel_id=1, replica_groups=mesh['fs'=16,'tp'=2] {'fs'}, dimensions={0}, use_global_device_ids=true | all-gather | bytes 313344 | tf_op jit(solution)/shard_map/all_gather | solution.py:53
  33.4 21.9 %all-gather.2 = f32[16,12,768]{2,1,0:T(8,128)S(1)} all-gather(f32[1,12,768]{2,1,0:T(8,128)} %bitcast.16), channel_id=1, replica_groups=mesh['fs'=16,'tp'=2] {'fs'}, dimensions={0}, use_global_device_ids=true | all-gather | bytes 626688 | tf_op jit(solution)/shard_map/all_gather | solution.py:55
  55.4 21.1 %all-gather.3 = f32[16,12,768]{2,1,0:T(8,128)S(1)} all-gather(f32[1,12,768]{2,1,0:T(8,128)S(1)} %bitcast.17), channel_id=1, replica_groups=mesh['fs'=16,'tp'=2] {'fs'}, dimensions={0}, use_global_device_ids=true | all-gather | bytes 626688 | tf_op jit(solution)/shard_map/all_gather | solution.py:56
  76.6 6.6 %fusion.1 = f32[192,768]{1,0:T(8,128)} fusion(bf16[1024,768]{1,0:T(8,128)(2,1)S(1)} %copy-done, bf16[1024,3072]{1,0:T(8,128)(2,1)} %param.11, bf16[3072,192]{1,0:T(8,128)(2,1)} %all-gather.11.cloned.1.call-done), kind=kOutput, calls=%fused_computation.5 | convolution fusion | flops 1510146048 | bytes 9633792 | tf_op jit(solution)/shard_map/dot_general | solution.py:48
  83.3 15.3 %all-gather.9.cloned.1.call-done = bf16[3072,192]{1,0:T(8,128)(2,1)} async-done(((bf16[192,192]{1,0:T(8,128)(2,1)}), bf16[3072,192]{1,0:T(8,128)(2,1)}) %all-gather.9.cloned.1.call-update) | async-done | bytes 1179664 | tf_op jit(solution)/shard_map/all_gather | solution.py:38
  98.5 6.5 %fusion = f32[192,384]{1,0:T(8,128)} fusion(bf16[1024,384]{1,0:T(8,128)(2,1)} %param.12, bf16[1024,3072]{1,0:T(8,128)(2,1)} %param.11, bf16[3072,192]{1,0:T(8,128)(2,1)} %all-gather.9.cloned.1.call-done), kind=kOutput, calls=%fused_computation.4 | convolution fusion | flops 1359151104 | bytes 8552448 | tf_op jit(solution)/shard_map/dot_general | solution.py:45
  105.0 2.1 pad_maximum_fusion
  107.2 0.8 broadcast_multiply_fusion.3
  108.0 0.9 reshape.33
  108.9 0.9 reshape.35
  110.0 0.7 reshape.29
  110.7 20.7 %all-gather.1 = f32[16,12,384]{2,1,0:T(8,128)S(1)} all-gather(f32[1,12,384]{2,1,0:T(8,128)S(1)} %bitcast.19), channel_id=1, replica_groups=mesh['fs'=16,'tp'=2] {'fs'}, dimensions={0}, use_global_device_ids=true | all-gather | bytes 313344 | tf_op jit(solution)/shard_map/all_gather | solution.py:54
  131.4 0.7 reshape.31
  132.2 67.6 %all-reduce.2.cloned.1.call-done = f32[192,1152]{1,0:T(8,128)} async-done(((f32[192,1152]{1,0:T(8,128)}), f32[192,1152]{1,0:T(8,128)}) %all-reduce.2.cloned.1.call-update) | async-done | bytes 884752 | tf_op jit(solution)/shard_map/psum | solution.py:51
  199.7 2.2 multiply_reduce_fusion
  202.0 1.8 multiply_reduce_fusion.1
  205.1 5.4 %psum.15 = f32[]{:T(128)} all-reduce(f32[]{:T(128)S(6)} %add.48), channel_id=1, replica_groups=mesh['fs'=16,'tp'=2] {'tp'}, use_global_device_ids=true, to_apply=%region_3.0 | all-reduce | flops 1 | bytes 8 | tf_op jit(solution)/shard_map/psum | solution.py:60
  211.2 2.1 fusion.7
  213.4 2.6 fusion.6
  217.3 37.5 %all-gather.13.cloned.1.call-done = bf16[3072,384]{1,0:T(8,128)(2,1)} async-done(((bf16[192,384]{1,0:T(8,128)(2,1)}), bf16[3072,384]{1,0:T(8,128)(2,1)}) %all-gather.13.cloned.1.call-update) | async-done | bytes 2359312 | tf_op jit(solution)/shard_map/all_gather | solution.py:74
  254.8 54.6 %all-gather.15.cloned.1.call-done = bf16[3072,768]{1,0:T(8,128)(2,1)} async-done(((bf16[192,768]{1,0:T(8,128)(2,1)}), bf16[3072,768]{1,0:T(8,128)(2,1)}) %all-gather.15.cloned.1.call-update) | async-done | bytes 4718608 | tf_op jit(solution)/shard_map/all_gather | solution.py:75
  309.4 3.5 %copy.24 = bf16[3072,384]{1,0:T(8,128)(2,1)} copy(bf16[3072,384]{1,0:T(8,128)(2,1)} %all-gather.13.cloned.1.call-done) | data formatting | bytes 4718592
  312.8 2.2 copy.25
  (35 shorter events, 2.6 us)
Async XLA Ops:
  7.2 69.5 %copy-start = (bf16[1024,768]{1,0:T(8,128)(2,1)S(1)}, bf16[1024,768]{1,0:T(8,128)(2,1)}, u32[]{:S(2)}) copy-start(bf16[1024,768]{1,0:T(8,128)(2,1)} %param.13) | copy-start | bytes 4718596
  7.2 48.2 %copy-start.8 = (f32[12,768]{1,0:T(8,128)S(1)}, f32[12,768]{1,0:T(8,128)}, u32[]{:S(2)}) copy-start(f32[12,768]{1,0:T(8,128)} %param.21) | copy-start | bytes 110596
  7.2 69.4 %all-gather.11.cloned.1.call-start = ((), (), s32[]{:S(2)}) async-start(), calls=%async_computation.1 | async-start | bytes 1671168 | tf_op jit(solution)/shard_map/all_gather | solution.py:39
  7.9 90.6 %all-gather.9.cloned.1.call-start = ((), (), s32[]{:S(2)}) async-start(), calls=%async_computation | async-start | bytes 1671168 | tf_op jit(solution)/shard_map/all_gather | solution.py:38
  8.7 191.0 %all-reduce.2.cloned.1.call-start = ((), (), s32[]{:S(2)}) async-start(), calls=%async_computation.2 | async-start | bytes 1769472 | tf_op jit(solution)/shard_map/psum | solution.py:51
  107.2 147.6 %all-gather.13.cloned.1.call-start = ((), (), s32[]{:S(2)}) async-start(), calls=%async_computation.3 | async-start | bytes 2506752 | tf_op jit(solution)/shard_map/all_gather | solution.py:74
  108.9 1.1 copy-start.3
  108.9 1.8 copy-start.9
  110.0 89.8 %copy-start.2 = (f32[192,768]{1,0:T(8,128)S(1)}, f32[192,768]{1,0:T(8,128)}, u32[]{:S(2)}) copy-start(f32[192,768]{1,0:T(8,128)} %reshape.33) | copy-start | bytes 1769476
  132.2 79.0 %copy-start.7 = (bf16[192,192]{1,0:T(8,128)(2,1)S(1)}, bf16[192,192]{1,0:T(8,128)(2,1)}, u32[]{:S(2)}) copy-start(bf16[192,192]{1,0:T(8,128)(2,1)} %param.14) | copy-start | bytes 221188
  199.7 2.2 copy-start.4
  199.7 2.2 copy-start.5
  202.0 11.4 %copy-start.6 = (bf16[192,192]{1,0:T(8,128)(2,1)S(1)}, bf16[192,192]{1,0:T(8,128)(2,1)}, u32[]{:S(2)}) copy-start(bf16[192,192]{1,0:T(8,128)(2,1)} %param.15) | copy-start | bytes 221188
  213.3 96.0 %all-gather.15.cloned.1.call-start = ((), (), s32[]{:S(2)}) async-start(), calls=%async_computation.4 | async-start | bytes 5013504 | tf_op jit(solution)/shard_map/all_gather | solution.py:75
  309.4 3.5 %copy-start.1 = (bf16[3072,768]{1,0:T(8,128)(2,1)S(1)}, bf16[3072,768]{1,0:T(8,128)(2,1)}, u32[]{:S(2)}) copy-start(bf16[3072,768]{1,0:T(8,128)(2,1)} %all-gather.15.cloned.1.call-done) | copy-start | bytes 14155780
Sparse Core Ops, SparseCore 0:
  10.3 43.8 all-gather.10
  56.4 42.0 all-gather.8
  107.3 92.3 all-reduce.1
  213.5 41.3 all-gather.12
  257.5 51.8 all-gather.14
where the time goes:
time: 322 us
  waiting for transfers between devices  176 us (55%)
  blocking collectives  93.8 us (29%)
  matrix products  17.9 us (6%)
  between operations  15.9 us (5%)
  local copies, waits for them, and re-layouts  10.4 us (3%)
  other arithmetic  7.08 us (2%)
    psum x1, waiting for transfers between devices, on_device(): full_sums = lax.psum(jnp.concatenate([term_q, term_v], axis=1), 'fs')  67.6 us
    all_gather x1, waiting for transfers between devices, on_device(): lax.all_gather(new_v.astype(jnp.bfloat16), 'fs', axis=0, tiled=True)  54.6 us
    all_gather x1, waiting for transfers between devices, on_device(): lax.all_gather(new_q.astype(jnp.bfloat16), 'fs', axis=0, tiled=True)  37.5 us
    all_gather x1, blocking collectives, on_device(): lax.all_gather(query_first, 'fs', axis=0, tiled=True)  24.6 us
    all_gather x1, blocking collectives, on_device(): lax.all_gather(value_first, 'fs', axis=0, tiled=True)  21.9 us
    all_gather x1, blocking collectives, on_device(): lax.all_gather(value_second, 'fs', axis=0, tiled=True)  21.1 us
    all_gather x1, blocking collectives, on_device(): lax.all_gather(query_second, 'fs', axis=0, tiled=True)  20.7 us
    all_gather x1, waiting for transfers between devices, on_device(): lax.all_gather(query_factor, 'fs', axis=0, tiled=True)  15.3 us
  transfers between devices with their start and end apart: 5, of which 4 were waited for; matrix products, arithmetic and copies ran while one was open for 5% of the time, Pallas kernels for 0%

commit v1 on v0

v1 whole, which is shorter than its diff:
```python
import functools

import jax
import jax.numpy as jnp
from jax import lax
from jax.experimental import pallas as pl
from jax.experimental.pallas import tpu as pltpu
from jax.sharding import PartitionSpec as P

first_decay = 0.9
second_decay = 0.99
small_eps = 1e-08
learn_rate = 0.01
CORES = 2
COLS = 2


def moments(old_first, old_second, gradient):
    first = first_decay * old_first + (1.0 - first_decay) * gradient
    second = second_decay * old_second + (1.0 - second_decay) * gradient * gradient
    unit = first / (jnp.sqrt(second) + small_eps)
    return (first, second, unit)


class Place:
    def __init__(self, n, t):
        self.n, self.t = n, t
        self.depth = n // (COLS * CORES)
        self.me = lax.axis_index("fs")
        self.tp = lax.axis_index("tp")
        self.c = self.me % CORES
        self.y = (self.me // CORES) % COLS
        self.z = self.me // (CORES * COLS)

    def at(self, z, y, c):
        return (z * COLS + y) * CORES + c

    def up(self, k):
        return (self.z + k) % self.depth

    def down(self, k):
        return (self.z + self.depth - k) % self.depth


class Gather:
    def __init__(self, place, own, full, sems):
        self.p, self.own, self.full = place, own, full
        self.zs, self.zr, self.ys, self.yr, self.cs, self.cr = sems
        self.sent = []

    def _copy(self, src, slot, ss, rs, to):
        return pltpu.make_async_remote_copy(
            src_ref=src, dst_ref=self.full.at[slot], send_sem=ss, recv_sem=rs,
            device_id={"fs": to}, device_id_type=pl.DeviceIdType.MESH)

    def _go(self, copy):
        copy.start()
        self.sent.append(copy)

    def piece(self, k):
        slot = self.p.at(self.p.down(k), self.p.y, self.p.c)
        return slot, (self.own if k == 0 else self.full.at[slot])

    def send_z(self, k):
        p = self.p
        self._go(self._copy(self.own, p.me, self.zs.at[k], self.zr.at[k], p.at(p.up(k), p.y, p.c)))

    def wait_z(self, k):
        slot = self.p.at(self.p.down(k), self.p.y, self.p.c)
        self._copy(self.full.at[slot], slot, self.zs.at[k], self.zr.at[k], self.p.me).wait_recv()

    def send_yc(self, k):
        p = self.p
        slot, src = self.piece(k)
        self._go(self._copy(src, slot, self.ys.at[k], self.yr.at[k], p.at(p.z, 1 - p.y, p.c)))
        self._go(self._copy(src, slot, self.cs.at[0, k], self.cr.at[0, k], p.at(p.z, p.y, 1 - p.c)))

    def pass_y(self, k):
        p = self.p
        slot = p.at(p.down(k), 1 - p.y, p.c)
        got = self.full.at[slot]
        self._copy(got, slot, self.ys.at[k], self.yr.at[k], p.me).wait_recv()
        self._go(self._copy(got, slot, self.cs.at[1, k], self.cr.at[1, k], p.at(p.z, p.y, 1 - p.c)))

    def wait_c(self):
        p = self.p
        for j in range(2):
            for k in range(p.depth):
                slot = p.at(p.down(k), p.y if j == 0 else 1 - p.y, 1 - p.c)
                self._copy(self.full.at[slot], slot, self.cs.at[j, k], self.cr.at[j, k], p.me).wait_recv()

    def drain(self):
        for copy in self.sent:
            copy.wait_send()


def gather_sems(depth):
    dma = pltpu.SemaphoreType.DMA
    return [dma((depth,)), dma((depth,)), dma((depth,)), dma((depth,)), dma((2, depth)), dma((2, depth))]


def kernel(
    n, t, x_hbm, cq_hbm, cv_hbm, f_own, w_own, q1, q2, v1, v2,
    w_all, f_all, bits, first_q, second_q, first_v, second_v,
    x, cq, cv, g, gc_in, gs, gy_in, gt, gz_in, u_own, u_all, u_flat, sq, sq_in,
    acc_q, acc_v, local, gsem, tsem, *sems):
    p = Place(n, t)
    depth = p.depth
    rows = q1.shape[0]
    rank, q_cols = acc_q.shape
    v_cols = acc_v.shape[1]
    F = Gather(p, f_own, f_all, sems[0:6])
    W = Gather(p, w_own, w_all, sems[6:12])
    U = Gather(p, u_own, u_all, sems[12:18])
    loads = [
        pltpu.make_async_copy(x_hbm, x, local.at[0]),
        pltpu.make_async_copy(cq_hbm, cq, local.at[1]),
        pltpu.make_async_copy(cv_hbm, cv, local.at[2]),
    ]
    for copy in loads:
        copy.start()
    keep = pltpu.make_async_copy(w_own, w_all.at[p.me], local.at[3])
    keep.start()

    barrier = pltpu.get_barrier_semaphore()
    peers = [{"fs": p.at(p.up(k), p.y, p.c)} for k in range(1, depth)]
    peers += [{"fs": p.at(p.z, 1 - p.y, p.c)}, {"fs": p.at(p.z, p.y, 1 - p.c)}]
    peers += [{"tp": (p.tp + k) % t} for k in range(1, t)]
    for peer in peers:
        pl.semaphore_signal(barrier, inc=1, device_id=peer, device_id_type=pl.DeviceIdType.MESH)
    pl.semaphore_wait(barrier, len(peers))

    for k in range(1, depth):
        F.send_z(k)
    F.send_yc(0)
    f_all[p.me] = f_own[...]
    for k in range(1, depth):
        F.wait_z(k)
        F.send_yc(k)
    W.send_yc(0)
    W.send_z(1)
    for k in range(depth):
        F.pass_y(k)
    F.wait_c()
    for copy in loads:
        copy.wait()

    acc_q[...] = jnp.zeros_like(acc_q)
    acc_v[...] = jnp.zeros_like(acc_v)
    tile = 256

    @pl.loop(0, x.shape[0] // tile)
    def _(i):
        at = pl.ds(pl.multiple_of(i * tile, tile), tile)
        f = f_all[...].reshape(x.shape[1], 2 * rank)
        proj = jnp.dot(x[at, :], f, preferred_element_type=jnp.float32)
        turned = proj.T.astype(jnp.bfloat16)
        acc_q[...] += jnp.dot(turned[:rank], cq[at, :], preferred_element_type=jnp.float32)
        acc_v[...] += jnp.dot(turned[rank:], cv[at, :], preferred_element_type=jnp.float32)

    for j in range(n):
        c, y, z = j % CORES, (j // CORES) % COLS, j // (CORES * COLS)
        g[c, y, z, :, :q_cols] = acc_q[j * rows:(j + 1) * rows, :]
        g[c, y, z, :, q_cols:] = acc_v[j * rows:(j + 1) * rows, :]

    def swap(src, dst, k, peer):
        return pltpu.make_async_remote_copy(
            src_ref=src, dst_ref=dst, send_sem=gsem.at[0, k], recv_sem=gsem.at[1, k],
            device_id=peer, device_id_type=pl.DeviceIdType.MESH)

    to_core = swap(g.at[1 - p.c], gc_in, 0, {"fs": p.at(p.z, p.y, 1 - p.c)})
    to_core.start()
    to_core.wait()
    gs[...] = g[p.c] + gc_in[...]
    to_col = swap(gs.at[1 - p.y], gy_in, depth, {"fs": p.at(p.z, 1 - p.y, p.c)})
    to_col.start()
    W.wait_z(1)
    to_col.wait()
    gt[...] = gs[p.y] + gy_in[...]
    to_z = [swap(gt.at[p.up(k)], gz_in.at[k - 1], k, {"fs": p.at(p.up(k), p.y, p.c)}) for k in range(1, depth)]
    for copy in to_z:
        copy.start()
    W.send_yc(1)
    total = gt[p.z]
    for k, copy in enumerate(to_z):
        copy.wait()
        total = total + gz_in[k]
    a1, a2, uq = moments(q1[...], q2[...], total[:, :q_cols])
    b1, b2, uv = moments(v1[...], v2[...], total[:, q_cols:])
    u_own[:, :q_cols] = uq
    u_own[:, q_cols:] = uv
    for k in range(1, depth):
        U.send_z(k)
    U.send_yc(0)
    for k in range(2, depth):
        W.send_z(k)
    first_q[...] = a1
    second_q[...] = a2
    first_v[...] = b1
    second_v[...] = b2
    u_all[p.me] = u_own[...]
    for k in range(1, depth):
        U.wait_z(k)
        U.send_yc(k)
    for k in range(depth):
        U.pass_y(k)
    U.wait_c()
    for j in range(n):
        u_flat[j * rows:(j + 1) * rows, :] = u_all[j]
    own_sq = jnp.sum(u_flat[...] * u_flat[...])
    sq[...] = jnp.full(sq.shape, own_sq, jnp.float32)
    shares = [
        pltpu.make_async_remote_copy(
            src_ref=sq, dst_ref=sq_in.at[k - 1], send_sem=tsem.at[0, k], recv_sem=tsem.at[1, k],
            device_id={"tp": (p.tp + k) % t}, device_id_type=pl.DeviceIdType.MESH)
        for k in range(1, t)
    ]
    for copy in shares:
        copy.start()
    for k in range(2, depth):
        W.wait_z(k)
        W.send_yc(k)
    norm = sq[...]
    for k, copy in enumerate(shares):
        copy.wait()
        norm = norm + sq_in[k]
    entries = rank * (q_cols + v_cols) * t
    scale = lax.rsqrt(norm[:1, :1] / entries + 1e-06)
    bits[...] = (scale * u_flat[...]).astype(jnp.bfloat16)
    for k in range(depth):
        W.pass_y(k)
    W.wait_c()
    keep.wait()
    F.drain()
    U.drain()
    W.drain()


def exchange(inputs, query_cot, value_cot, f_own, w_own, query_first, query_second, value_first, value_second):
    n, t = lax.axis_size("fs"), lax.axis_size("tp")
    depth = n // (COLS * CORES)
    rows, q_cols = query_first.shape
    v_cols = value_first.shape[1]
    cols = q_cols + v_cols
    rank = rows * n
    any_, vmem = pl.BlockSpec(memory_space=pl.ANY), pl.BlockSpec(memory_space=pltpu.VMEM)
    f32, bf16 = jnp.float32, jnp.bfloat16
    dma = pltpu.SemaphoreType.DMA
    shape = jax.ShapeDtypeStruct
    return pl.pallas_call(
        functools.partial(kernel, n, t),
        out_shape=(
            shape((n,) + w_own.shape, bf16), shape((n,) + f_own.shape, bf16), shape((rank, cols), bf16),
            shape((rows, q_cols), f32), shape((rows, q_cols), f32),
            shape((rows, v_cols), f32), shape((rows, v_cols), f32),
        ),
        in_specs=[any_] * 3 + [vmem] * 6,
        out_specs=(any_,) + (vmem,) * 6,
        scratch_shapes=[
            pltpu.VMEM(inputs.shape, bf16), pltpu.VMEM(query_cot.shape, bf16), pltpu.VMEM(value_cot.shape, bf16),
            pltpu.VMEM((CORES, COLS, depth, rows, cols), f32), pltpu.VMEM((COLS, depth, rows, cols), f32),
            pltpu.VMEM((COLS, depth, rows, cols), f32), pltpu.VMEM((depth, rows, cols), f32),
            pltpu.VMEM((depth, rows, cols), f32), pltpu.VMEM((depth - 1, rows, cols), f32),
            pltpu.VMEM((rows, cols), f32), pltpu.VMEM((n, rows, cols), f32), pltpu.VMEM((rank, cols), f32),
            pltpu.VMEM((8, 128), f32), pltpu.VMEM((t - 1, 8, 128), f32),
            pltpu.VMEM((rank, q_cols), f32), pltpu.VMEM((rank, v_cols), f32),
            dma((4,)), dma((2, depth + 1)), dma((2, t)),
        ] + gather_sems(depth) * 3,
        compiler_params=pltpu.CompilerParams(
            collective_id=0, has_side_effects=True, vmem_limit_bytes=48 * 1024 * 1024),
    )(inputs, query_cot, value_cot, f_own, w_own, query_first, query_second, value_first, value_second)


def by_collectives(inputs, query_cot, value_cot, f_own, w_own, query_first, query_second, value_first, value_second):
    q_cols = query_cot.shape[1]
    n, rank = lax.axis_size("fs"), f_own.shape[1] // 2
    entries = rank * (q_cols + value_cot.shape[1]) * lax.axis_size("tp")
    f_all = lax.all_gather(f_own, "fs", axis=0)
    w_all = lax.all_gather(w_own, "fs", axis=0)
    proj = jnp.dot(inputs, f_all.reshape(-1, 2 * rank), preferred_element_type=jnp.float32).astype(jnp.bfloat16)
    over = (((0,), (0,)), ((), ()))
    term_q = lax.dot_general(proj[:, :rank], query_cot, over, preferred_element_type=jnp.float32)
    term_v = lax.dot_general(proj[:, rank:], value_cot, over, preferred_element_type=jnp.float32)
    own = lax.psum_scatter(jnp.concatenate([term_q, term_v], axis=1), "fs", scatter_dimension=0, tiled=True)
    first_q, second_q, unit_q = moments(query_first, query_second, own[:, :q_cols])
    first_v, second_v, unit_v = moments(value_first, value_second, own[:, q_cols:])
    total = lax.psum(jnp.sum(unit_q * unit_q) + jnp.sum(unit_v * unit_v), ("fs", "tp"))
    scale = lax.rsqrt(total / entries + 1e-06)
    mine = (scale * jnp.concatenate([unit_q, unit_v], axis=1)).astype(jnp.bfloat16)
    bits = lax.all_gather(mine, "fs", axis=0, tiled=True)
    return w_all, f_all, bits, first_q, second_q, first_v, second_v


def on_device(
    inputs, query_cot, value_cot, query_factor, value_factor, query_weight, value_weight,
    query_first, query_second, value_first, value_second,
):
    n = lax.axis_size("fs")
    rank, q_cols, v_cols = query_factor.shape[1], query_cot.shape[1], value_cot.shape[1]
    f_own = jnp.concatenate([query_factor, value_factor], axis=1)
    w_own = jnp.concatenate([query_weight, value_weight], axis=1).astype(jnp.bfloat16)
    whole = (
        n % (COLS * CORES) == 0 and n > COLS * CORES and lax.axis_size("tp") > 1 and q_cols % 128 == 0
        and v_cols % 128 == 0 and (2 * rank) % 128 == 0 and inputs.shape[1] % 128 == 0
        and inputs.shape[0] % 256 == 0 and query_factor.shape[0] % 16 == 0 and rank % 16 == 0
    )
    run = exchange if whole else by_collectives
    w_all, f_all, bits, first_q, second_q, first_v, second_v = run(
        inputs, query_cot, value_cot, f_own, w_own, query_first, query_second, value_first, value_second)
    f_full = f_all.reshape(-1, 2 * rank)
    w_full = w_all.reshape(-1, q_cols + v_cols)
    bits_q, bits_v = bits[:, :q_cols], bits[:, q_cols:]
    f32 = jnp.float32
    step_q = jnp.dot(query_factor, bits_q, preferred_element_type=f32)
    step_v = jnp.dot(value_factor, bits_v, preferred_element_type=f32)
    new_q = query_weight - learn_rate * step_q
    new_v = value_weight - learn_rate * step_v
    all_q = jnp.dot(f_full[:, :rank], bits_q, preferred_element_type=f32)
    all_v = jnp.dot(f_full[:, rank:], bits_v, preferred_element_type=f32)
    copy_q = (w_full[:, :q_cols].astype(f32) - learn_rate * all_q).astype(jnp.bfloat16)
    copy_v = (w_full[:, q_cols:].astype(f32) - learn_rate * all_v).astype(jnp.bfloat16)
    return (step_q, step_v, new_q, new_v, first_q, second_q, first_v, second_v, copy_q, copy_v)


def solution(mesh):
    row, both = P("fs", None), P("fs", "tp")
    in_specs = (row, both, both, row, row) + (both,) * 6
    out_specs = (both,) * 8 + (P(None, "tp"),) * 2
    return jax.shard_map(on_device, mesh=mesh, in_specs=in_specs, out_specs=out_specs, check_vma=False)
```

time: 322 us -> 131 us (0.41)
  the two profiles are of different devices: /device:TPU:0 before, /device:TPU:27 now
where the time goes in v1:
time: 131 us
  Pallas kernels  108 us (82%)
  matrix products  11.2 us (9%)
  local copies, waits for them, and re-layouts  8.07 us (6%)
  other arithmetic  3.16 us (2%)
    pallas_call x1, Pallas kernels, exchange(): pl.pallas_call(functools.partial(kernel, n, t), out_shape=(shape((n,) + w...  108 us
    unnamed x24, local copies, waits for them, and re-layouts  8.07 us
    dot_general x1, matrix products, on_device(): all_v = jnp.dot(f_full[:, rank:], bits_v, preferred_element_type=f32)  4.8 us
    dot_general x1, matrix products, on_device(): all_q = jnp.dot(f_full[:, :rank], bits_q, preferred_element_type=f32)  4.13 us

profile of v1, /device:TPU:27, one launch (start us, length us, event | category | flops | bytes accessed | tf_op | source)
XLA Modules:
  0.0 130.7 jit_solution(18216019880246709166)
XLA Ops:
  0.6 1.1 convert.7
  1.7 1.0 convert.6
  2.8 1.0 pad_maximum_fusion.1.f_own
  3.8 0.0 copy-start
  3.8 1.4 %copy-done = bf16[1024,768]{1,0:T(8,128)(2,1)S(1)} copy-done((bf16[1024,768]{1,0:T(8,128)(2,1)S(1)}, bf16[1024,768]{1,0:T(8,128)(2,1)}, u32[]{:S(2)}) %copy-start) | copy-done | bytes 1572888
  5.2 0.0 copy-start.1
  5.2 1.1 copy-done.1
  6.4 0.8 copy-done.2
  7.2 0.8 copy-done.3
  8.0 0.7 copy-done.4
  8.7 0.7 copy-done.5
  9.4 107.6 %shard_map.186 = (bf16[16,192,1152]{2,1,0:T(8,128)(2,1)}, bf16[16,192,384]{2,1,0:T(8,128)(2,1)S(1)}, bf16[192,1152]{1,0:T(8,128)(2,1)S(1)}, f32[12,384]{1,0:T(8,...) custom-call(bf16[1024,3072]{1,0:T(8,128)(2,1)} %x_hbm.1, ...), custom_call_target="tpu_custom_call" | custom-call | tf_op jit(solution)/shard_map/pallas_call | solution.py:250
  117.0 4.8 %subtract_convert_fusion = bf16[3072,768]{1,0:T(8,128)(2,1)} fusion(bf16[3072,1152]{1,0:T(8,128)(2,1)} %bitcast.10, bf16[3072,384]{1,0:T(8,128)(2,1)S(1)} %bitcast.8, bf16[192,1152]{1,0:T(8,128)(2,1)S(1)} %get-tuple-element.17), kind=kOutput, calls=%fused_computation | convolution fusion | flops 915406848 | bytes 11304960 | tf_op jit(solution)/shard_map/dot_general | solution.py:319
  121.8 4.1 %subtract_convert_fusion.1 = bf16[3072,384]{1,0:T(8,128)(2,1)} fusion(bf16[3072,1152]{1,0:T(8,128)(2,1)} %bitcast.11, bf16[3072,384]{1,0:T(8,128)(2,1)S(1)} %bitcast.9, bf16[192,1152]{1,0:T(8,128)(2,1)S(1)} %get-tuple-element.17), kind=kOutput, calls=%fused_computation.1 | convolution fusion | flops 457703424 | bytes 6438912 | tf_op jit(solution)/shard_map/dot_general | solution.py:318
  126.0 0.0 copy-done.6
  126.0 0.0 copy-done.8
  126.0 1.2 multiply_subtract_fusion
  127.2 0.0 copy-done.7
  127.2 0.0 copy-done.9
  127.2 1.0 multiply_subtract_fusion.1
  128.2 0.6 copy.25
  128.8 0.6 copy.26
  129.5 0.6 copy.27
  130.1 0.6 copy.28
  (9 shorter events, 0.1 us)
Async XLA Ops:
  3.8 1.4 %copy-start = (bf16[1024,768]{1,0:T(8,128)(2,1)S(1)}, bf16[1024,768]{1,0:T(8,128)(2,1)}, u32[]{:S(2)}) copy-start(bf16[1024,768]{1,0:T(8,128)(2,1)} %cv_hbm.1) | copy-start | bytes 4718596
  5.2 1.1 copy-start.1
  6.4 0.8 copy-start.2
  7.2 0.8 copy-start.3
  8.0 0.7 copy-start.4
  8.7 0.7 copy-start.5
  121.8 4.1 %copy-start.6 = (f32[192,768]{1,0:T(8,128)S(1)}, f32[192,768]{1,0:T(8,128)}, u32[]{:S(2)}) copy-start(f32[192,768]{1,0:T(8,128)} %param.17) | copy-start | bytes 1769476
  121.8 4.1 %copy-start.8 = (bf16[192,192]{1,0:T(8,128)(2,1)S(1)}, bf16[192,192]{1,0:T(8,128)(2,1)}, u32[]{:S(2)}) copy-start(bf16[192,192]{1,0:T(8,128)(2,1)} %param.15) | copy-start | bytes 221188
  121.8 5.4 %copy-start.7 = (f32[192,384]{1,0:T(8,128)S(1)}, f32[192,384]{1,0:T(8,128)}, u32[]{:S(2)}) copy-start(f32[192,384]{1,0:T(8,128)} %param.16) | copy-start | bytes 884740
  121.8 5.4 %copy-start.9 = (bf16[192,192]{1,0:T(8,128)(2,1)S(1)}, bf16[192,192]{1,0:T(8,128)(2,1)}, u32[]{:S(2)}) copy-start(bf16[192,192]{1,0:T(8,128)(2,1)} %param.14) | copy-start | bytes 221188

commit v2 on v1

--- a/solution.py
+++ b/solution.py
@@ -99,10 +99,118 @@
     return [dma((depth,)), dma((depth,)), dma((depth,)), dma((depth,)), dma((2, depth)), dma((2, depth))]
 
 
+class Line:
+    def __init__(self, place, own, full, sems):
+        self.p, self.own, self.full = place, own, full
+        self.zs, self.zr, self.ys, self.yr, self.cs, self.cr = sems
+        self.sent = []
+
+    def _copy(self, src, slot, ss, rs, to):
+        return pltpu.make_async_remote_copy(
+            src_ref=src, dst_ref=self.full.at[slot], send_sem=ss, recv_sem=rs,
+            device_id={"fs": to}, device_id_type=pl.DeviceIdType.MESH)
+
+    def _go(self, when, make):
+        pl.when(when)(lambda: make().start())
+        self.sent.append((when, make))
+
+    def origin(self, d, s):
+        z = self.p.z - 1 - s if d == 0 else self.p.z + 1 + s
+        return z, (z >= 0 if d == 0 else z < self.p.depth)
+
+    def send(self, s):
+        p = self.p
+        for d in range(2):
+            to, frm = (p.z + 1, p.z - s) if d == 0 else (p.z - 1, p.z + s)
+            when = jnp.logical_and(to < p.depth, frm >= 0) if d == 0 else jnp.logical_and(to >= 0, frm < p.depth)
+
+            def make(d=d, to=to, frm=frm):
+                slot = p.at(frm, p.y, p.c)
+                src = self.own if s == 0 else self.full.at[slot]
+                return self._copy(src, slot, self.zs.at[d, s], self.zr.at[d, s], p.at(to, p.y, p.c))
+
+            self._go(when, make)
+
+    def wait(self, s):
+        p = self.p
+        for d in range(2):
+            z, when = self.origin(d, s)
+
+            @pl.when(when)
+            def _(d=d, z=z):
+                slot = p.at(z, p.y, p.c)
+                self._copy(self.full.at[slot], slot, self.zs.at[d, s], self.zr.at[d, s], p.me).wait_recv()
+
+    def own_yc(self):
+        p, k = self.p, self.p.depth - 1
+        self._go(True, lambda: self._copy(
+            self.own, p.me, self.ys.at[0, k], self.yr.at[0, k], p.at(p.z, 1 - p.y, p.c)))
+        self._go(True, lambda: self._copy(
+            self.own, p.me, self.cs.at[0, 0, k], self.cr.at[0, 0, k], p.at(p.z, p.y, 1 - p.c)))
+
+    def forward(self, d, s, also=True):
+        p = self.p
+        z, when = self.origin(d, s)
+        when = jnp.logical_and(when, also)
+
+        def to_y():
+            slot = p.at(z, p.y, p.c)
+            return self._copy(self.full.at[slot], slot, self.ys.at[d, s], self.yr.at[d, s], p.at(p.z, 1 - p.y, p.c))
+
+        def to_c():
+            slot = p.at(z, p.y, p.c)
+            return self._copy(
+                self.full.at[slot], slot, self.cs.at[0, d, s], self.cr.at[0, d, s], p.at(p.z, p.y, 1 - p.c))
+
+        self._go(when, to_y)
+        self._go(when, to_c)
+
+    def items(self):
+        last = self.p.depth - 1
+        yield 0, last, self.p.z, True
+        for s in range(last):
+            for d in range(2):
+                z, when = self.origin(d, s)
+                yield d, s, z, when
+
+    def pass_y(self):
+        p = self.p
+        for d, s, z, when in self.items():
+            slot = p.at(z, 1 - p.y, p.c)
+
+            @pl.when(when)
+            def _(d=d, s=s, slot=slot):
+                got = self.full.at[slot]
+                self._copy(got, slot, self.ys.at[d, s], self.yr.at[d, s], p.me).wait_recv()
+
+            self._go(when, lambda d=d, s=s, slot=slot: self._copy(
+                self.full.at[slot], slot, self.cs.at[1, d, s], self.cr.at[1, d, s], p.at(p.z, p.y, 1 - p.c)))
+
+    def wait_c(self):
+        p = self.p
+        for j in range(2):
+            for d, s, z, when in self.items():
+                slot = p.at(z, p.y if j == 0 else 1 - p.y, 1 - p.c)
+
+                @pl.when(when)
+                def _(d=d, s=s, slot=slot):
+                    self._copy(self.full.at[slot], slot, self.cs.at[j, d, s], self.cr.at[j, d, s], p.me).wait_recv()
+
+    def drain(self):
+        for when, make in self.sent:
+            pl.when(when)(lambda make=make: make().wait_send())
+
+
+def line_sems(depth):
+    dma = pltpu.SemaphoreType.DMA
+    return [dma((2, depth))] * 4 + [dma((2, 2, depth))] * 2
+
+
 def kernel(
-    n, t, x_hbm, cq_hbm, cv_hbm, f_own, w_own, q1, q2, v1, v2,
-    w_all, f_all, bits, first_q, second_q, first_v, second_v,
-    x, cq, cv, g, gc_in, gs, gy_in, gt, gz_in, u_own, u_all, u_flat, sq, sq_in,
+    n, t, x_hbm, cq_hbm, cv_hbm, qf_hbm, vf_hbm, qw_hbm, vw_hbm, q1_hbm, q2_hbm, v1_hbm, v2_hbm,
+    w_all, f_all, bits, grad,
+    x, cq, cv, qf, vf, qw, vw, q1, q2, v1, v2,
+    f_own, w_own, g, gc_in, gs, gy_in, gt, gz_in, u_own, u_all, u_flat, sq, sq_in,
     acc_q, acc_v, local, gsem, tsem, *sems):
     p = Place(n, t)
     depth = p.depth
@@ -110,17 +218,14 @@
     rank, q_cols = acc_q.shape
     v_cols = acc_v.shape[1]
     F = Gather(p, f_own, f_all, sems[0:6])
-    W = Gather(p, w_own, w_all, sems[6:12])
+    W = Line(p, w_own, w_all, sems[6:12])
     U = Gather(p, u_own, u_all, sems[12:18])
-    loads = [
-        pltpu.make_async_copy(x_hbm, x, local.at[0]),
-        pltpu.make_async_copy(cq_hbm, cq, local.at[1]),
-        pltpu.make_async_copy(cv_hbm, cv, local.at[2]),
-    ]
+    pairs = (
+        (qf_hbm, qf), (vf_hbm, vf), (qw_hbm, qw), (vw_hbm, vw), (x_hbm, x), (cq_hbm, cq), (cv_hbm, cv),
+        (q1_hbm, q1), (q2_hbm, q2), (v1_hbm, v1), (v2_hbm, v2))
+    loads = [pltpu.make_async_copy(src, dst, local.at[i]) for i, (src, dst) in enumerate(pairs)]
     for copy in loads:
         copy.start()
-    keep = pltpu.make_async_copy(w_own, w_all.at[p.me], local.at[3])
-    keep.start()
 
     barrier = pltpu.get_barrier_semaphore()
     peers = [{"fs": p.at(p.up(k), p.y, p.c)} for k in range(1, depth)]
@@ -128,21 +233,30 @@
     peers += [{"tp": (p.tp + k) % t} for k in range(1, t)]
     for peer in peers:
         pl.semaphore_signal(barrier, inc=1, device_id=peer, device_id_type=pl.DeviceIdType.MESH)
+    loads[0].wait()
+    loads[1].wait()
+    f_own[:, :rank] = qf[...]
+    f_own[:, rank:] = vf[...]
     pl.semaphore_wait(barrier, len(peers))
 
     for k in range(1, depth):
         F.send_z(k)
     F.send_yc(0)
     f_all[p.me] = f_own[...]
+    loads[2].wait()
+    loads[3].wait()
+    w_own[:, :q_cols] = qw[...].astype(jnp.bfloat16)
+    w_own[:, q_cols:] = vw[...].astype(jnp.bfloat16)
+    w_all[p.me] = w_own[...]
     for k in range(1, depth):
         F.wait_z(k)
         F.send_yc(k)
-    W.send_yc(0)
-    W.send_z(1)
+    W.own_yc()
+    W.send(0)
     for k in range(depth):
         F.pass_y(k)
     F.wait_c()
-    for copy in loads:
+    for copy in loads[4:]:
         copy.wait()
 
     acc_q[...] = jnp.zeros_like(acc_q)
@@ -170,38 +284,40 @@
 
     to_core = swap(g.at[1 - p.c], gc_in, 0, {"fs": p.at(p.z, p.y, 1 - p.c)})
     to_core.start()
+    W.wait(0)
+    W.send(1)
     to_core.wait()
     gs[...] = g[p.c] + gc_in[...]
     to_col = swap(gs.at[1 - p.y], gy_in, depth, {"fs": p.at(p.z, 1 - p.y, p.c)})
     to_col.start()
-    W.wait_z(1)
+    W.forward(0, 0)
+    W.forward(1, 0, p.z == 0)
     to_col.wait()
     gt[...] = gs[p.y] + gy_in[...]
     to_z = [swap(gt.at[p.up(k)], gz_in.at[k - 1], k, {"fs": p.at(p.up(k), p.y, p.c)}) for k in range(1, depth)]
     for copy in to_z:
         copy.start()
-    W.send_yc(1)
     total = gt[p.z]
     for k, copy in enumerate(to_z):
         copy.wait()
         total = total + gz_in[k]
-    a1, a2, uq = moments(q1[...], q2[...], total[:, :q_cols])
-    b1, b2, uv = moments(v1[...], v2[...], total[:, q_cols:])
-    u_own[:, :q_cols] = uq
-    u_own[:, q_cols:] = uv
+    grad[...] = total
+    u_own[:, :q_cols] = moments(q1[...], q2[...], total[:, :q_cols])[2]
+    u_own[:, q_cols:] = moments(v1[...], v2[...], total[:, q_cols:])[2]
     for k in range(1, depth):
         U.send_z(k)
     U.send_yc(0)
-    for k in range(2, depth):
-        W.send_z(k)
-    first_q[...] = a1
-    second_q[...] = a2
-    first_v[...] = b1
-    second_v[...] = b2
-    u_all[p.me] = u_own[...]
-    for k in range(1, depth):
-        U.wait_z(k)
-        U.send_yc(k)
+    for s in range(1, depth - 2):
+        W.wait(s)
+        W.send(s + 1)
+        if s == 1:
+            u_all[p.me] = u_own[...]
+            for k in range(1, depth):
+                U.wait_z(k)
+                U.send_yc(k)
+            W.forward(1, 0, p.z > 0)
+        for d in range(2):
+            W.forward(d, s)
     for k in range(depth):
         U.pass_y(k)
     U.wait_c()
@@ -217,9 +333,9 @@
     ]
     for copy in shares:
         copy.start()
-    for k in range(2, depth):
-        W.wait_z(k)
-        W.send_yc(k)
+    W.wait(depth - 2)
+    for d in range(2):
+        W.forward(d, depth - 2)
     norm = sq[...]
     for k, copy in enumerate(shares):
         copy.wait()
@@ -227,51 +343,57 @@
     entries = rank * (q_cols + v_cols) * t
     scale = lax.rsqrt(norm[:1, :1] / entries + 1e-06)
     bits[...] = (scale * u_flat[...]).astype(jnp.bfloat16)
-    for k in range(depth):
-        W.pass_y(k)
+    W.pass_y()
     W.wait_c()
-    keep.wait()
     F.drain()
     U.drain()
     W.drain()
 
 
-def exchange(inputs, query_cot, value_cot, f_own, w_own, query_first, query_second, value_first, value_second):
+def exchange(*args):
+    inputs, query_cot, value_cot, query_factor, value_factor, query_weight, value_weight = args[:7]
     n, t = lax.axis_size("fs"), lax.axis_size("tp")
     depth = n // (COLS * CORES)
-    rows, q_cols = query_first.shape
-    v_cols = value_first.shape[1]
+    rows, q_cols = args[7].shape
+    v_cols = args[9].shape[1]
     cols = q_cols + v_cols
-    rank = rows * n
+    rank, deep = rows * n, query_factor.shape[0]
     any_, vmem = pl.BlockSpec(memory_space=pl.ANY), pl.BlockSpec(memory_space=pltpu.VMEM)
     f32, bf16 = jnp.float32, jnp.bfloat16
     dma = pltpu.SemaphoreType.DMA
     shape = jax.ShapeDtypeStruct
-    return pl.pallas_call(
+    w_all, f_all, bits, grad = pl.pallas_call(
         functools.partial(kernel, n, t),
         out_shape=(
-            shape((n,) + w_own.shape, bf16), shape((n,) + f_own.shape, bf16), shape((rank, cols), bf16),
-            shape((rows, q_cols), f32), shape((rows, q_cols), f32),
-            shape((rows, v_cols), f32), shape((rows, v_cols), f32),
+            shape((n, deep, cols), bf16), shape((n, deep, 2 * rank), bf16), shape((rank, cols), bf16),
+            shape((rows, cols), f32),
         ),
-        in_specs=[any_] * 3 + [vmem] * 6,
-        out_specs=(any_,) + (vmem,) * 6,
-        scratch_shapes=[
-            pltpu.VMEM(inputs.shape, bf16), pltpu.VMEM(query_cot.shape, bf16), pltpu.VMEM(value_cot.shape, bf16),
+        in_specs=[any_] * len(args),
+        out_specs=(vmem,) * 4,
+        scratch_shapes=[pltpu.VMEM(a.shape, a.dtype) for a in args] + [
+            pltpu.VMEM((deep, 2 * rank), bf16), pltpu.VMEM((deep, cols), bf16),
             pltpu.VMEM((CORES, COLS, depth, rows, cols), f32), pltpu.VMEM((COLS, depth, rows, cols), f32),
             pltpu.VMEM((COLS, depth, rows, cols), f32), pltpu.VMEM((depth, rows, cols), f32),
             pltpu.VMEM((depth, rows, cols), f32), pltpu.VMEM((depth - 1, rows, cols), f32),
             pltpu.VMEM((rows, cols), f32), pltpu.VMEM((n, rows, cols), f32), pltpu.VMEM((rank, cols), f32),
             pltpu.VMEM((8, 128), f32), pltpu.VMEM((t - 1, 8, 128), f32),
             pltpu.VMEM((rank, q_cols), f32), pltpu.VMEM((rank, v_cols), f32),
-            dma((4,)), dma((2, depth + 1)), dma((2, t)),
-        ] + gather_sems(depth) * 3,
+            dma((len(args),)), dma((2, depth + 1)), dma((2, t)),
+        ] + gather_sems(depth) + line_sems(depth) + gather_sems(depth),
         compiler_params=pltpu.CompilerParams(
-            collective_id=0, has_side_effects=True, vmem_limit_bytes=48 * 1024 * 1024),
-    )(inputs, query_cot, value_cot, f_own, w_own, query_first, query_second, value_first, value_second)
-
-
-def by_collectives(inputs, query_cot, value_cot, f_own, w_own, query_first, query_second, value_first, value_second):
+            collective_id=0, has_side_effects=True, vmem_limit_bytes=52 * 1024 * 1024),
+    )(*args)
+    first_q, second_q, _ = moments(args[7], args[8], grad[:, :q_cols])
+    first_v, second_v, _ = moments(args[9], args[10], grad[:, q_cols:])
+    return w_all, f_all, bits, first_q, second_q, first_v, second_v
+
+
+def by_collectives(
+    inputs, query_cot, value_cot, query_factor, value_factor, query_weight, value_weight,
+    query_first, query_second, value_first, value_second,
+):
+    f_own = jnp.concatenate([query_factor, value_factor], axis=1)
+    w_own = jnp.concatenate([query_weight, value_weight], axis=1).astype(jnp.bfloat16)
     q_cols = query_cot.shape[1]
     n, rank = lax.axis_size("fs"), f_own.shape[1] // 2
     entries = rank * (q_cols + value_cot.shape[1]) * lax.axis_size("tp")
@@ -297,16 +419,15 @@
 ):
     n = lax.axis_size("fs")
     rank, q_cols, v_cols = query_factor.shape[1], query_cot.shape[1], value_cot.shape[1]
-    f_own = jnp.concatenate([query_factor, value_factor], axis=1)
-    w_own = jnp.concatenate([query_weight, value_weight], axis=1).astype(jnp.bfloat16)
     whole = (
-        n % (COLS * CORES) == 0 and n > COLS * CORES and lax.axis_size("tp") > 1 and q_cols % 128 == 0
+        n % (COLS * CORES) == 0 and n >= 4 * COLS * CORES and lax.axis_size("tp") > 1 and q_cols % 128 == 0
         and v_cols % 128 == 0 and (2 * rank) % 128 == 0 and inputs.shape[1] % 128 == 0
         and inputs.shape[0] % 256 == 0 and query_factor.shape[0] % 16 == 0 and rank % 16 == 0
     )
     run = exchange if whole else by_collectives
     w_all, f_all, bits, first_q, second_q, first_v, second_v = run(
-        inputs, query_cot, value_cot, f_own, w_own, query_first, query_second, value_first, value_second)
+        inputs, query_cot, value_cot, query_factor, value_factor, query_weight, value_weight,
+        query_first, query_second, value_first, value_second)
     f_full = f_all.reshape(-1, 2 * rank)
     w_full = w_all.reshape(-1, q_cols + v_cols)
     bits_q, bits_v = bits[:, :q_cols], bits[:, q_cols:]

time: 131 us -> 111 us (0.85)
  the two profiles are of different devices: /device:TPU:27 before, /device:TPU:0 now
where the time goes in v2:
time: 111 us; the launch traced here: 110 us
  Pallas kernels  88.1 us (79%)
  matrix products  13.1 us (12%)
  local copies, waits for them, and re-layouts  6.88 us (6%)
  other arithmetic  1.28 us (1%)
    pallas_call x1, Pallas kernels, exchange(): pl.pallas_call(functools.partial(kernel, n, t), out_shape=(shape((n, deep...  88.1 us
    unnamed x18, local copies, waits for them, and re-layouts  6.88 us
    dot_general x1, matrix products, on_device(): all_v = jnp.dot(f_full[:, rank:], bits_v, preferred_element_type=f32)  6.79 us
    dot_general x1, matrix products, on_device(): all_q = jnp.dot(f_full[:, :rank], bits_q, preferred_element_type=f32)  4.05 us

profile of v2, /device:TPU:0, one launch (start us, length us, event | category | flops | bytes accessed | tf_op | source)
XLA Modules:
  0.0 110.0 jit_solution(10826987490679326425)
XLA Ops:
  0.6 0.0 copy-start
  0.7 1.1 copy-done
  1.7 0.0 copy-start.1
  1.7 1.0 copy-done.1
  2.7 0.0 copy-start.2
  2.7 0.9 copy-done.2
  3.6 0.0 copy-start.3
  3.6 0.9 copy-done.3
  4.5 0.0 copy-start.4
  4.5 0.8 copy-done.4
  5.3 0.0 copy-start.5
  5.3 0.8 copy-done.5
  6.1 0.0 copy-start.6
  6.1 0.7 copy-done.6
  6.8 0.7 copy-done.7
  7.5 88.1 %shard_map.186 = (bf16[16,192,1152]{2,1,0:T(8,128)(2,1)}, bf16[16,192,384]{2,1,0:T(8,128)(2,1)}, bf16[192,1152]{1,0:T(8,128)(2,1)S(1)}, f32[12,1152]{1,0:T(8,128)S(1)}) custom-call(bf16[1024,3072]{1,0:T(8,128)(2,1)} %x_hbm.1, bf16[1024,384]{1,0:T(8,128)(2,1)} %cq_hbm.1, bf16[1024,768]{1,0:T(8,128)(2,1)} %cv_hbm.1, bf16[192,192]{1,0:T(8,128)(2,1)S(1)} %copy-done.3, ...), custom_call_target="tpu_custom_call" | custom-call | tf_op jit(solution)/shard_map/pallas_call | solution.py:365
  95.6 0.0 copy-start.8
  95.6 6.8 %subtract_convert_fusion = bf16[3072,768]{1,0:T(8,128)(2,1)} fusion(bf16[3072,1152]{1,0:T(8,128)(2,1)} %bitcast.8, bf16[3072,384]{1,0:T(8,128)(2,1)} %bitcast.10, bf16[192,1152]{1,0:T(8,128)(2,1)S(1)} %get-tuple-element.14), kind=kOutput, calls=%fused_computation | convolution fusion | flops 915406848 | bytes 11304960 | tf_op jit(solution)/shard_map/dot_general | solution.py:440
  102.4 0.0 copy-done.8
  102.4 4.0 %subtract_convert_fusion.1 = bf16[3072,384]{1,0:T(8,128)(2,1)} fusion(bf16[3072,1152]{1,0:T(8,128)(2,1)} %bitcast.9, bf16[3072,384]{1,0:T(8,128)(2,1)S(1)} %bitcast.11, bf16[192,1152]{1,0:T(8,128)(2,1)S(1)} %get-tuple-element.14), kind=kOutput, calls=%fused_computation.1 | convolution fusion | flops 457703424 | bytes 6438912 | tf_op jit(solution)/shard_map/dot_general | solution.py:439
  106.5 1.2 %multiply_subtract_fusion = (f32[192,768]{1,0:T(8,128)}, f32[192,768]{1,0:T(8,128)}) fusion(f32[192,768]{1,0:T(8,128)S(1)} %copy-done, bf16[192,192]{1,0:T(8,128)(2,1)S(1)} %copy-done.2, bf16[192,1152]{1,0:T(8,128)(2,1)S(1)} %get-tuple-element.14), kind=kOutput, calls=%fused_computation.6 | convolution fusion | flops 56918016 | bytes 2162688 | tf_op jit(solution)/shard_map/dot_general | solution.py:436
  107.7 1.0 multiply_subtract_fusion.1
  108.7 0.7 fusion.6
  109.4 0.6 fusion.7
  (1 shorter events, 0.0 us)
Async XLA Ops:
  0.6 1.1 copy-start
  1.7 1.0 copy-start.1
  2.7 0.9 copy-start.2
  3.6 0.9 copy-start.3
  4.5 0.8 copy-start.4
  5.3 0.8 copy-start.5
  6.1 0.7 copy-start.6
  6.8 0.7 copy-start.7
  95.6 6.8 %copy-start.8 = (bf16[16,192,384]{2,1,0:T(8,128)(2,1)S(1)}, bf16[16,192,384]{2,1,0:T(8,128)(2,1)}, u32[]{:S(2)}) copy-start(bf16[16,192,384]{2,1,0:T(8,128)(2,1)} %get-tuple-element.17) | copy-start | bytes 7077892

commit v3 on v2

--- a/solution.py
+++ b/solution.py
@@ -381,7 +381,7 @@
             dma((len(args),)), dma((2, depth + 1)), dma((2, t)),
         ] + gather_sems(depth) + line_sems(depth) + gather_sems(depth),
         compiler_params=pltpu.CompilerParams(
-            collective_id=0, has_side_effects=True, vmem_limit_bytes=52 * 1024 * 1024),
+            collective_id=0, has_side_effects=True, vmem_limit_bytes=54 * 1024 * 1024 - 65536),
     )(*args)
     first_q, second_q, _ = moments(args[7], args[8], grad[:, :q_cols])
     first_v, second_v, _ = moments(args[9], args[10], grad[:, q_cols:])
@@ -413,6 +413,37 @@
     return w_all, f_all, bits, first_q, second_q, first_v, second_v
 
 
+def copy_kernel(w, f, bits, copy_q, copy_v):
+    rank, q_cols = f.shape[2] // 2, copy_q.shape[1]
+    for i in range(w.shape[0]):
+        deep = w.shape[1]
+        at = slice(i * deep, (i + 1) * deep)
+        step_q = jnp.dot(f[i][:, :rank], bits[:, :q_cols], preferred_element_type=jnp.float32)
+        step_v = jnp.dot(f[i][:, rank:], bits[:, q_cols:], preferred_element_type=jnp.float32)
+        copy_q[at, :] = (w[i][:, :q_cols].astype(jnp.float32) - learn_rate * step_q).astype(jnp.bfloat16)
+        copy_v[at, :] = (w[i][:, q_cols:].astype(jnp.float32) - learn_rate * step_v).astype(jnp.bfloat16)
+
+
+def copies(w_all, f_all, bits, q_cols):
+    n, deep, cols = w_all.shape
+    some = 2
+    shape = jax.ShapeDtypeStruct
+    return pl.pallas_call(
+        copy_kernel,
+        grid=(n // some,),
+        out_shape=(shape((n * deep, q_cols), jnp.bfloat16), shape((n * deep, cols - q_cols), jnp.bfloat16)),
+        in_specs=[
+            pl.BlockSpec((some, deep, cols), lambda i: (i, 0, 0)),
+            pl.BlockSpec((some,) + f_all.shape[1:], lambda i: (i, 0, 0)),
+            pl.BlockSpec(bits.shape, lambda i: (0, 0)),
+        ],
+        out_specs=(
+            pl.BlockSpec((some * deep, q_cols), lambda i: (i, 0)),
+            pl.BlockSpec((some * deep, cols - q_cols), lambda i: (i, 0)),
+        ),
+    )(w_all, f_all, bits)
+
+
 def on_device(
     inputs, query_cot, value_cot, query_factor, value_factor, query_weight, value_weight,
     query_first, query_second, value_first, value_second,
@@ -428,6 +459,13 @@
     w_all, f_all, bits, first_q, second_q, first_v, second_v = run(
         inputs, query_cot, value_cot, query_factor, value_factor, query_weight, value_weight,
         query_first, query_second, value_first, value_second)
+    if whole:
+        step_q = jnp.dot(query_factor, bits[:, :q_cols], preferred_element_type=jnp.float32)
+        step_v = jnp.dot(value_factor, bits[:, q_cols:], preferred_element_type=jnp.float32)
+        new_q = query_weight - learn_rate * step_q
+        new_v = value_weight - learn_rate * step_v
+        copy_q, copy_v = copies(w_all, f_all, bits, q_cols)
+        return (step_q, step_v, new_q, new_v, first_q, second_q, first_v, second_v, copy_q, copy_v)
     f_full = f_all.reshape(-1, 2 * rank)
     w_full = w_all.reshape(-1, q_cols + v_cols)
     bits_q, bits_v = bits[:, :q_cols], bits[:, q_cols:]

time: 111 us -> 103 us (0.928)
  matrix products: 13.1 us -> 2.25 us
  Pallas kernels: 88.1 us -> 98 us
  local copies, waits for them, and re-layouts: 6.88 us -> 0.06 us
    dot_general x4 -> x2, matrix products: 13.1 us -> 2.25 us  [the longest x1 1.24 us: on_device(): jnp.dot(value_factor, bits[:, q_cols:], preferred_element_type=jnp.float32)]
    pallas_call x0 -> x1, Pallas kernels: none -> 10.3 us  [copies(): pl.pallas_call(copy_kernel, grid=(n // some,), out_shape=(shape((n * deep...]
    unnamed x18 -> x20, local copies, waits for them, and re-layouts: 6.88 us -> 0.06 us
where the time goes in v3:
time: 103 us; the launch traced here: 102 us
  Pallas kernels  98 us (95%)
  matrix products  2.25 us (2%)
  other arithmetic  1.28 us (1%)
    pallas_call x1, Pallas kernels, exchange(): pl.pallas_call(functools.partial(kernel, n, t), out_shape=(shape((n, deep...  87.7 us
    pallas_call x1, Pallas kernels, copies(): pl.pallas_call(copy_kernel, grid=(n // some,), out_shape=(shape((n * deep...  10.3 us

profile of v3, /device:TPU:0, one launch (start us, length us, event | category | flops | bytes accessed | tf_op | source)
XLA Modules:
  0.0 102.3 jit_solution(11880445770452402021)
XLA Ops:
  0.6 87.7 %shard_map.186 = (bf16[16,192,1152]{2,1,0:T(8,128)(2,1)}, bf16[16,192,384]{2,1,0:T(8,128)(2,1)}, bf16[192,1152]{1,0:T(8,128)(2,1)}, f32[12,1152]{1,0:T(8,128)}) custom-call(bf16[1024,3072]{1,0:T(8,128)(2,1)} %x_hbm.1, bf16[1024,384]{1,0:T(8,128)(2,1)} %cq_hbm.1, bf16[1024,768]{1,0:T(8,128)(2,1)} %cv_hbm.1, bf16[192,192]{1,0:T(8,128)(2,1)} %qf_hbm.1, ...), custom_call_target="tpu_custom_call" | custom-call | tf_op jit(solution)/shard_map/pallas_call | solution.py:365
  88.3 0.0 copy-start.7
  88.4 0.0 copy-start.8
  88.4 0.0 copy-start.9
  88.4 0.0 copy-start.5
  88.4 0.0 copy-start.6
  88.4 0.0 copy-start.1
  88.4 0.0 copy-start.2
  88.4 0.0 copy-start.4
  88.4 0.0 copy-start
  88.5 0.0 copy-start.3
  88.5 10.3 %shard_map.187 = (bf16[3072,384]{1,0:T(8,128)(2,1)}, bf16[3072,768]{1,0:T(8,128)(2,1)}) custom-call(bf16[16,192,1152]{2,1,0:T(8,128)(2,1)} %get-tuple-element.18.w, bf16[16,192,384]{2,1,0:T(8,128)(2,1)} %get-tuple-element.19.f, bf16[192,1152]{1,0:T(8,128)(2,1)} %get-tuple-element.16.bits), custom_call_target="tpu_custom_call" | custom-call | tf_op jit(solution)/shard_map/pallas_call | solution.py:431
  98.7 0.0 copy-done.7
  98.8 0.0 copy-done.8
  98.8 0.0 copy-done.9
  98.8 0.6 fusion.3
  99.4 0.0 copy-done.5
  99.4 0.0 copy-done.6
  99.4 0.7 fusion.2
  100.1 0.0 copy-done.1
  100.1 0.0 copy-done.2
  100.1 0.0 copy-done.4
  100.1 1.0 multiply_subtract_fusion.1
  101.1 1.2 %multiply_subtract_fusion = (f32[192,768]{1,0:T(8,128)}, f32[192,768]{1,0:T(8,128)}) fusion(f32[192,768]{1,0:T(8,128)S(1)} %copy-done, bf16[192,192]{1,0:T(8,128)(2,1)S(1)} %copy-done.3, bf16[192,1152]{1,0:T(8,128)(2,1)S(1)} %copy-done.1), kind=kOutput, calls=%fused_computation.2 | convolution fusion | flops 56918016 | bytes 2162688 | tf_op jit(solution)/shard_map/dot_general | solution.py:464
  (2 shorter events, 0.0 us)
Async XLA Ops:
  88.3 10.4 %copy-start.7 = (f32[12,384]{1,0:T(8,128)S(1)}, f32[12,384]{1,0:T(8,128)}, u32[]{:S(2)}) copy-start(f32[12,384]{1,0:T(8,128)} %q1_hbm.1) | copy-start | bytes 55300
  88.4 10.4 %copy-start.8 = (f32[12,384]{1,0:T(8,128)S(1)}, f32[12,384]{1,0:T(8,128)}, u32[]{:S(2)}) copy-start(f32[12,384]{1,0:T(8,128)} %q2_hbm.1) | copy-start | bytes 55300
  88.4 10.4 %copy-start.9 = (f32[12,1152]{1,0:T(8,128)S(1)}, f32[12,1152]{1,0:T(8,128)}, u32[]{:S(2)}) copy-start(f32[12,1152]{1,0:T(8,128)} %get-tuple-element.17) | copy-start | bytes 165892
  88.4 11.0 %copy-start.5 = (f32[12,768]{1,0:T(8,128)S(1)}, f32[12,768]{1,0:T(8,128)}, u32[]{:S(2)}) copy-start(f32[12,768]{1,0:T(8,128)} %v1_hbm.1) | copy-start | bytes 110596
  88.4 11.0 %copy-start.6 = (f32[12,768]{1,0:T(8,128)S(1)}, f32[12,768]{1,0:T(8,128)}, u32[]{:S(2)}) copy-start(f32[12,768]{1,0:T(8,128)} %v2_hbm.1) | copy-start | bytes 110596
  88.4 11.6 %copy-start.1 = (bf16[192,1152]{1,0:T(8,128)(2,1)S(1)}, bf16[192,1152]{1,0:T(8,128)(2,1)}, u32[]{:S(2)}) copy-start(bf16[192,1152]{1,0:T(8,128)(2,1)} %get-tuple-element.16.bits) | copy-start | bytes 1327108
  88.4 11.6 %copy-start.2 = (f32[192,384]{1,0:T(8,128)S(1)}, f32[192,384]{1,0:T(8,128)}, u32[]{:S(2)}) copy-start(f32[192,384]{1,0:T(8,128)} %qw_hbm.1) | copy-start | bytes 884740
  88.4 11.6 %copy-start.4 = (bf16[192,192]{1,0:T(8,128)(2,1)S(1)}, bf16[192,192]{1,0:T(8,128)(2,1)}, u32[]{:S(2)}) copy-start(bf16[192,192]{1,0:T(8,128)(2,1)} %qf_hbm.1) | copy-start | bytes 221188
  88.4 12.6 %copy-start = (f32[192,768]{1,0:T(8,128)S(1)}, f32[192,768]{1,0:T(8,128)}, u32[]{:S(2)}) copy-start(f32[192,768]{1,0:T(8,128)} %vw_hbm.1) | copy-start | bytes 1769476
  88.5 12.6 %copy-start.3 = (bf16[192,192]{1,0:T(8,128)(2,1)S(1)}, bf16[192,192]{1,0:T(8,128)(2,1)}, u32[]{:S(2)}) copy-start(bf16[192,192]{1,0:T(8,128)(2,1)} %vf_hbm.1) | copy-start | bytes 221188
